TPU v7x, 32 devices: a whole 2x2x4 slice. The times are simulated.
32 devices in a mesh: grp: 2 (over y), kv: 4 (over z), tp: 4 (over x, core).
Axes of the slice: x: 2, y: 2, z: 4, core: 2. Of those that a mesh axis runs over, the one named last changes fastest.
Arguments:
- tokens: bfloat16 [16, 4096], P('grp', 'kv'), parts along dimension 0, may hold values from -6 to 6
- norm_gain: float32 [4096], replicated, may hold values from 0.1 to 1.9
- w_query: bfloat16 [4096, 4096], P('kv', 'tp'), may hold values from -0.09375 to 0.09375
- key_weight: bfloat16 [4096, 512], P('kv', 'tp'), may hold values from -0.09375 to 0.09375
- value_weight: bfloat16 [4096, 512], P('kv', 'tp'), may hold values from -0.09375 to 0.09375
- w_gate: bfloat16 [4096, 64], replicated, may hold values from -0.09375 to 0.09375
- gate_bias: float32 [64], replicated, may hold values from -3 to 4
- w_out: bfloat16 [4096, 4096], P('kv', 'tp'), may hold values from -0.1875 to 0.1875
- cache_keys: bfloat16 [16, 3072, 512], P('grp', 'kv', 'tp'), parts along dimension 0, may hold values from -240 to 240
- cache_values: bfloat16 [16, 3072, 512], P('grp', 'kv', 'tp'), parts along dimension 0, may hold values from -8 to 8
- cache_gate: float32 [16, 64, 3072], P('grp', 'tp', 'kv'), parts along dimension 0, may hold values from -3072 to 0, as said below
- gate_total: float32 [16, 64], P('grp', 'tp'), parts along dimension 0, may hold values from -3072 to 0, as said below
- lengths: int32 [16], P('grp'), parts along dimension 0, may hold values from 1536 to 3072, as said below
Outputs:
- mixed: bfloat16 [16, 4096], P('grp', 'kv'), parts along dimension 0
- key_new: bfloat16 [16, 512], P('grp', 'tp'), parts along dimension 0
- value_new: bfloat16 [16, 512], P('grp', 'tp'), parts along dimension 0
There are 2 independent parts, one for each index of `grp`. A program takes and returns all parts, laid end to end along the dimension named above; an argument that names none is the same for every part. Nothing has to cross between parts.
Inputs may be any that keep to these rules, and one draw needn't show every extreme that they name: `lengths`: one sequence of each draw has all 3072 positions cached. `cache_gate`: non-increasing along positions. `gate_total`: equal to cache_gate at position lengths - 1 of the same sequence and head.
All inputs are finite; a program needn't handle non-finite values.
Results may differ from a plain program's by a relative error of at most 0.015.
Values may be sent and summed in bfloat16 or wider, within the bound.
A program may use at most 64 MiB of HBM per device.

v0:
```python
import jax
import jax.numpy as jnp
from jax import lax
from jax.sharding import PartitionSpec as P

HEAD_SIZE = 64
NEG_FILL = -1e30


def per_device(
    tokens,
    norm_gain,
    w_query,
    key_weight,
    value_weight,
    w_gate,
    gate_bias,
    w_out,
    cache_keys,
    cache_values,
    cache_gate,
    gate_total,
    lengths,
):
    seq_count = tokens.shape[0]
    width_dev = tokens.shape[1]
    heads_dev = cache_gate.shape[1]
    positions_dev = cache_gate.shape[2]
    kv_heads_dev = cache_keys.shape[2] // HEAD_SIZE
    head_group = heads_dev // kv_heads_dev
    logit_scale = HEAD_SIZE ** (-0.5)
    whole = lax.all_gather(tokens, "kv", axis=1, tiled=True)
    features = whole.astype(jnp.float32)
    normed = (
        features
        * lax.rsqrt(jnp.mean(features * features, axis=-1, keepdims=True) + 1e-06)
        * norm_gain
    )
    normed = normed.astype(jnp.bfloat16)
    kv_index = lax.axis_index("kv")
    tp_index = lax.axis_index("tp")
    own_rows = lax.dynamic_slice_in_dim(normed, kv_index * width_dev, width_dev, 1)
    query_part = jnp.dot(own_rows, w_query, preferred_element_type=jnp.float32)
    key_part = jnp.dot(own_rows, key_weight, preferred_element_type=jnp.float32)
    value_part = jnp.dot(own_rows, value_weight, preferred_element_type=jnp.float32)
    query_sum, key_sum, value_sum = lax.psum((query_part, key_part, value_part), "kv")
    query = query_sum.astype(jnp.bfloat16)
    key_new = key_sum.astype(jnp.bfloat16)
    value_new = value_sum.astype(jnp.bfloat16)
    gate_cols = lax.dynamic_slice_in_dim(w_gate, tp_index * heads_dev, heads_dev, 1)
    bias_cols = lax.dynamic_slice_in_dim(gate_bias, tp_index * heads_dev, heads_dev, 0)
    log_gate = jax.nn.log_sigmoid(
        jnp.dot(normed, gate_cols, preferred_element_type=jnp.float32) + bias_cols
    )
    level = gate_total + log_gate
    query_head_rows = query.reshape(seq_count, kv_heads_dev, head_group, HEAD_SIZE)
    key_block = cache_keys.reshape(seq_count, positions_dev, kv_heads_dev, HEAD_SIZE)
    value_block = cache_values.reshape(seq_count, positions_dev, kv_heads_dev, HEAD_SIZE)
    score_matrix = (
        jnp.einsum(
            "skgd,spkd->skgp", query_head_rows, key_block, preferred_element_type=jnp.float32
        )
        * logit_scale
    )
    forget_bias = (level[:, :, None] - cache_gate).reshape(
        seq_count, kv_heads_dev, head_group, positions_dev
    )
    positions = kv_index * positions_dev + jnp.arange(positions_dev, dtype=jnp.int32)
    valid_mask = (positions[None, :] < lengths[:, None])[:, None, None, :]
    score_matrix = jnp.where(valid_mask, score_matrix + forget_bias, NEG_FILL)
    local_max = jnp.max(score_matrix, axis=-1)
    weights = jnp.where(valid_mask, jnp.exp(score_matrix - local_max[..., None]), 0.0)
    local_total = jnp.sum(weights, axis=-1)
    local_values = jnp.einsum(
        "skgp,spkd->skgd",
        weights.astype(jnp.bfloat16),
        value_block,
        preferred_element_type=jnp.float32,
    )
    block_max = lax.pmax(local_max, "kv")
    rescale = jnp.exp(local_max - block_max)
    block_total, block_values = lax.psum(
        (local_total * rescale, local_values * rescale[..., None]), "kv"
    )
    key_current = key_new.reshape(seq_count, kv_heads_dev, HEAD_SIZE)
    current_score = (
        jnp.einsum(
            "skgd,skd->skg", query_head_rows, key_current, preferred_element_type=jnp.float32
        )
        * logit_scale
    )
    top = jnp.maximum(block_max, current_score)
    cached_scale = jnp.exp(block_max - top)
    current_weight = jnp.exp(current_score - top)
    denominator = block_total * cached_scale + current_weight
    value_current = value_new.reshape(seq_count, kv_heads_dev, 1, HEAD_SIZE).astype(jnp.float32)
    total_sum = block_values * cached_scale[..., None] + current_weight[..., None] * value_current
    attended = (
        (total_sum / denominator[..., None])
        .reshape(seq_count, heads_dev * HEAD_SIZE)
        .astype(jnp.bfloat16)
    )
    partial_value = lax.dot_general(
        attended, w_out, (((1,), (1,)), ((), ())), preferred_element_type=jnp.float32
    )
    partial_value = lax.optimization_barrier(partial_value.astype(jnp.bfloat16)).astype(jnp.float32)
    mixed = lax.psum(partial_value.astype(jnp.bfloat16), "tp")
    return (mixed, key_new, value_new)


def solution(mesh):
    placed = (
        P("grp", "kv"),
        P(),
        P("kv", "tp"),
        P("kv", "tp"),
        P("kv", "tp"),
        P(),
        P(),
        P("kv", "tp"),
        P("grp", "kv", "tp"),
        P("grp", "kv", "tp"),
        P("grp", "tp", "kv"),
        P("grp", "tp"),
        P("grp"),
    )
    return jax.shard_map(
        per_device,
        mesh=mesh,
        in_specs=placed,
        out_specs=(P("grp", "kv"), P("grp", "tp"), P("grp", "tp")),
        check_vma=False,
    )
```

profile of v0, /device:TPU:0, one launch (start us, length us, event | category | flops | bytes accessed | tf_op | source)
XLA Modules:
  0.0 91.3 jit_solution(11908319094124294041)
XLA Ops:
  0.7 0.9 dynamic_slice.11
  1.5 0.7 broadcast_compare_fusion
  2.3 15.1 %all_gather.3 = bf16[8,4096]{1,0:T(8,128)(2,1)S(1)} all-gather(bf16[8,1024]{1,0:T(8,128)(2,1)} %param.13), channel_id=1, replica_groups=mesh['grp'=2,'kv'=4,'tp'=4] {'kv'}, dimensions={1}, use_global_device_ids=true | all-gather | bytes 81920 | tf_op jit(solution)/shard_map/all_gather | solution.py:32
  17.4 0.1 fusion.9
  17.5 0.8 fusion.11
  18.4 1.1 %fusion.22 = f32[8,16]{1,0:T(8,128)S(1)} fusion(f32[8,16]{1,0:T(8,128)} %param.24, bf16[8,4096]{1,0:T(8,128)(2,1)S(1)} %fusion.11, bf16[4096,64]{0,1:T(8,128)(2,1)} %param.18, s32[]{:T(128)S(6)} %select_n.20, f32[16]{0:T(128)S(1)} %dynamic_slice.11), kind=kOutput, calls=%fused_computation.35 | convolution fusion | flops 1049856 | bytes 201284 | tf_op jit(solution)/shard_map/dot_general | solution.py:53
  19.4 1.1 %fusion.15 = f32[8,128]{1,0:T(8,128)S(1)} fusion(bf16[1024,128]{1,0:T(8,128)(2,1)} %param.16, bf16[8,4096]{1,0:T(8,128)(2,1)S(1)} %fusion.11, s32[]{:T(128)S(6)} %select_n.19), kind=kOutput, calls=%fused_computation.24 | convolution fusion | flops 2097152 | bytes 282628 | tf_op jit(solution)/shard_map/dot_general | solution.py:44
  20.6 1.1 %fusion.13 = f32[8,128]{1,0:T(8,128)S(1)} fusion(bf16[1024,128]{1,0:T(8,128)(2,1)} %param.17, bf16[8,4096]{1,0:T(8,128)(2,1)S(1)} %fusion.11, s32[]{:T(128)S(6)} %select_n.19), kind=kOutput, calls=%fused_computation.22 | convolution fusion | flops 2097152 | bytes 282628 | tf_op jit(solution)/shard_map/dot_general | solution.py:45
  21.7 0.4 fusion.17
  22.0 19.1 %psum.42 = bf16[8,1024]{1,0:T(8,128)(2,1)S(1)} all-reduce(f32[8,1024]{1,0:T(8,128)S(1)} %fusion.17), channel_id=1, replica_groups=mesh['grp'=2,'kv'=4,'tp'=4] {'kv'}, use_global_device_ids=true, to_apply=%region_1.0 | all-reduce | flops 8192 | bytes 49152 | tf_op jit(solution)/shard_map/psum | solution.py:46
  41.2 0.1 reshape.76
  41.3 2.7 %copy.18 = bf16[8,768,128]{1,2,0:T(8,128)(2,1)} copy(bf16[8,768,128]{2,1,0:T(8,128)(2,1)} %param.21) | data formatting | bytes 3145728 | tf_op args[8]
  43.9 1.8 %fusion.33 = (f32[8,2,8]{2,1,0:T(2,128)S(1)}, f32[8,2,8,768]{3,2,1,0:T(8,128)S(1)}) fusion(f32[8,16,768]{2,1,0:T(8,128)S(1)} %copy-done.1, f32[8,16]{1,0:T(8,128)S(1)} %fusion.22, bf16[8,2,8,64]{3,2,1,0:T(8,128)(2,1)S(1)} %reshape.76, bf16[8,768,2,64]{1,3,2,0:T(8,128)(2,1)} %bitcast.24, pred[8,768]{1,0:T(8,128)(4,1)S(1)} %broadcast_compare_fusion), kind=kOutput, calls=%fused_computation.44 | convolution fusion | flops 13074304 | bytes 2382848 | tf_op jit(solution)/shard_map/skgd,spkd->skgp/dot_general | solution.py:60
  45.7 8.5 %pmax.7 = f32[8,2,8]{2,1,0:T(2,128)S(1)} all-reduce(f32[8,2,8]{2,1,0:T(2,128)S(1)} %get-tuple-element.12), channel_id=1, replica_groups=mesh['grp'=2,'kv'=4,'tp'=4] {'kv'}, use_global_device_ids=true, to_apply=%region_3.0 | all-reduce | flops 128 | bytes 1024 | tf_op jit(solution)/shard_map/pmax | solution.py:80
  54.3 0.2 fusion.3
  54.5 2.6 %copy.19 = bf16[8,768,128]{1,2,0:T(8,128)(2,1)} copy(bf16[8,768,128]{2,1,0:T(8,128)(2,1)} %param.22) | data formatting | bytes 3145728 | tf_op args[9]
  57.1 2.0 %convolution_multiply_fusion.1 = f32[8,2,8,64]{3,2,1,0:T(8,128)S(1)} fusion(bf16[8,768,2,64]{1,3,2,0:T(8,128)(2,1)} %bitcast.25, f32[8,2,8,768]{3,2,1,0:T(8,128)S(1)} %get-tuple-element.13, f32[8,2,8]{2,1,0:T(2,128)S(1)} %get-tuple-element.12, pred[8,768]{1,0:T(8,128)(4,1)S(1)} %broadcast_compare_fusion, f32[8,2,8]{2,1,0:T(2,128)S(1)} %bitcast.30), kind=kOutput, calls=%fused_computation.3 | convolution fusion | flops 12886016 | bytes 2006016 | tf_op jit(solution)/shard_map/skgp,spkd->skgd/dot_general | solution.py:74
  59.1 18.7 %all-reduce = (f32[8,2,8,64]{3,2,1,0:T(8,128)S(1)}, bf16[8,128]{1,0:T(8,128)(2,1)S(1)}, f32[8,2,8]{2,1,0:T(2,128)S(1)}, bf16[8,128]{1,0:T(8,128)(2,1)S(1)}) all-reduce(f32[8,2,8,64]{3,2,1,0:T(8,128)S(1)} %convolution_multiply_fusion.1, f32[8,128]{1,0:T(8,128)S(1)} %fusion.15, ...), channel_id=1, replica_groups=mesh['grp'=2,'kv'=4,'tp'=4] {'kv'}, use_global_device_ids=true, to_apply=%region_4.5 | all-reduce | flops 10368 | bytes 78848 | tf_op jit(solution)/shard_map/psum | solution.py:82
  77.9 0.1 fusion.34
  78.1 0.1 reshape.81
  78.1 0.1 divide_convert_fusion
  78.3 0.1 convert_element_type.49
  78.4 2.2 %convolution_convert_fusion = bf16[8,1024]{1,0:T(8,128)(2,1)S(1)} fusion(bf16[8,1024]{1,0:T(8,128)(2,1)S(1)} %convert_element_type.49, bf16[1024,1024]{1,0:T(8,128)(2,1)} %param.20), kind=kOutput, calls=%fused_computation.4 | convolution fusion | flops 16785408 | bytes 2129920 | tf_op jit(solution)/shard_map/dot_general | solution.py:103
  80.6 10.7 %psum.47 = bf16[8,1024]{1,0:T(8,128)(2,1)} all-reduce(bf16[8,1024]{1,0:T(8,128)(2,1)S(1)} %convolution_convert_fusion), channel_id=1, replica_groups=mesh['grp'=2,'kv'=4,'tp'=4] {'tp'}, use_global_device_ids=true, to_apply=%region_9.10 | all-reduce | flops 8192 | bytes 32768 | tf_op jit(solution)/shard_map/psum | solution.py:107
  (13 shorter events, 0.2 us)
Async XLA Ops:
  0.6 21.0 %copy-start = (bf16[1024,1024]{1,0:T(8,128)(2,1)S(1)}, bf16[1024,1024]{1,0:T(8,128)(2,1)}, u32[]{:S(2)}) copy-start(bf16[1024,1024]{1,0:T(8,128)(2,1)} %param.15) | copy-start | bytes 6291460
  41.3 2.7 %copy-start.1 = (f32[8,16,768]{2,1,0:T(8,128)S(1)}, f32[8,16,768]{2,1,0:T(8,128)}, u32[]{:S(2)}) copy-start(f32[8,16,768]{2,1,0:T(8,128)} %param.23) | copy-start | bytes 1179652
  77.8 13.5 %copy-start.2 = (bf16[8,128]{1,0:T(8,128)(2,1)}, bf16[8,128]{1,0:T(8,128)(2,1)S(1)}, u32[]{:S(2)}) copy-start(bf16[8,128]{1,0:T(8,128)(2,1)S(1)} %get-tuple-element.4) | copy-start | bytes 6148
  77.8 13.5 %copy-start.3 = (bf16[8,128]{1,0:T(8,128)(2,1)}, bf16[8,128]{1,0:T(8,128)(2,1)S(1)}, u32[]{:S(2)}) copy-start(bf16[8,128]{1,0:T(8,128)(2,1)S(1)} %get-tuple-element.6) | copy-start | bytes 6148
where the time goes:
time: 91.8 us; the launch traced here: 91.3 us
  blocking collectives  72.2 us (79%)
  matrix products  9.82 us (11%)
  local copies, waits for them, and re-layouts  6.53 us (7%)
  other arithmetic  2.09 us (2%)
    psum x1, blocking collectives, per_device(): lax.psum((query_part, key_part, value_part), 'kv')  19.1 us
    psum x1, blocking collectives, per_device(): lax.psum((local_total * rescale, local_values * rescale[..., None]), 'kv')  18.7 us
    all_gather x1, blocking collectives, per_device(): whole = lax.all_gather(tokens, 'kv', axis=1, tiled=True)  15.1 us
    psum x1, blocking collectives, per_device(): mixed = lax.psum(partial_value.astype(jnp.bfloat16), 'tp')  10.7 us
    pmax x1, blocking collectives, per_device(): block_max = lax.pmax(local_max, 'kv')  8.5 us
    unnamed x10, local copies, waits for them, and re-layouts  5.29 us
    dot_general x1, matrix products, per_device(): lax.dot_general(attended, w_out, (((1,), (1,)), ((), ())), preferred_elem...  2.23 us
    dot_general x1, matrix products, per_device(): jnp.einsum('skgp,spkd->skgd', weights.astype(jnp.bfloat16), value_block,...  1.98 us

commit v1 on v0

--- a/solution.py
+++ b/solution.py
@@ -2,6 +2,7 @@
 import jax.numpy as jnp
 from jax import lax
 from jax.sharding import PartitionSpec as P
+from jax.lax import all_gather
 
 HEAD_SIZE = 64
 NEG_FILL = -1e30
@@ -104,7 +105,7 @@
         attended, w_out, (((1,), (1,)), ((), ())), preferred_element_type=jnp.float32
     )
     partial_value = lax.optimization_barrier(partial_value.astype(jnp.bfloat16)).astype(jnp.float32)
-    mixed = lax.psum(partial_value.astype(jnp.bfloat16), "tp")
+    mixed = jnp.sum(all_gather(partial_value.astype(jnp.bfloat16), "tp"), axis=0)
     return (mixed, key_new, value_new)
 
 

time: 91.8 us -> 87 us (0.948)
  blocking collectives: 72.2 us -> 66.7 us
    psum x1 -> x0, blocking collectives: 10.7 us -> none  [per_device(): mixed = lax.psum(partial_value.astype(jnp.bfloat16), 'tp')]
    all_gather x0 -> x1, blocking collectives: none -> 5.24 us  [per_device(): all_gather(partial_value.astype(jnp.bfloat16), 'tp')]
where the time goes in v1:
time: 87 us; the launch traced here: 86.5 us
  blocking collectives  66.7 us (77%)
  matrix products  9.82 us (11%)
  local copies, waits for them, and re-layouts  6.53 us (8%)
  other arithmetic  2.7 us (3%)
    psum x1, blocking collectives, per_device(): lax.psum((query_part, key_part, value_part), 'kv')  19.1 us
    psum x1, blocking collectives, per_device(): lax.psum((local_total * rescale, local_values * rescale[..., None]), 'kv')  18.7 us
    all_gather x1, blocking collectives, per_device(): whole = lax.all_gather(tokens, 'kv', axis=1, tiled=True)  15.1 us
    pmax x1, blocking collectives, per_device(): block_max = lax.pmax(local_max, 'kv')  8.5 us
    unnamed x10, local copies, waits for them, and re-layouts  5.29 us
    all_gather x1, blocking collectives, per_device(): all_gather(partial_value.astype(jnp.bfloat16), 'tp')  5.24 us
    dot_general x1, matrix products, per_device(): lax.dot_general(attended, w_out, (((1,), (1,)), ((), ())), preferred_elem...  2.23 us
    dot_general x1, matrix products, per_device(): jnp.einsum('skgp,spkd->skgd', weights.astype(jnp.bfloat16), value_block,...  1.98 us

profile of v1, /device:TPU:0, one launch (start us, length us, event | category | flops | bytes accessed | tf_op | source)
XLA Modules:
  0.0 86.5 jit_solution(10388174928833785122)
XLA Ops:
  0.7 0.9 %dynamic_slice.11 = f32[16]{0:T(128)S(1)} dynamic-slice(f32[64]{0:T(128)} %param.19, s32[]{:T(128)S(6)} %select_n.20), dynamic_slice_sizes={16} | dynamic-slice | bytes 132 | tf_op jit(solution)/shard_map/dynamic_slice | solution.py:52
  1.5 0.7 broadcast_compare_fusion
  2.3 15.1 %all_gather.9 = bf16[8,4096]{1,0:T(8,128)(2,1)S(1)} all-gather(bf16[8,1024]{1,0:T(8,128)(2,1)} %param.13), channel_id=1, replica_groups=mesh['grp'=2,'kv'=4,'tp'=4] {'kv'}, dimensions={1}, use_global_device_ids=true | all-gather | bytes 81920 | tf_op jit(solution)/shard_map/all_gather | solution.py:33
  17.4 0.1 fusion.9
  17.5 0.8 fusion.11
  18.4 1.1 %fusion.22 = f32[8,16]{1,0:T(8,128)S(1)} fusion(f32[8,16]{1,0:T(8,128)} %param.24, bf16[8,4096]{1,0:T(8,128)(2,1)S(1)} %fusion.11, bf16[4096,64]{0,1:T(8,128)(2,1)} %param.18, s32[]{:T(128)S(6)} %select_n.20, f32[16]{0:T(128)S(1)} %dynamic_slice.11), kind=kOutput, calls=%fused_computation.36 | convolution fusion | flops 1049856 | bytes 201284 | tf_op jit(solution)/shard_map/dot_general | solution.py:54
  19.4 1.1 %fusion.15 = f32[8,128]{1,0:T(8,128)S(1)} fusion(bf16[1024,128]{1,0:T(8,128)(2,1)} %param.16, bf16[8,4096]{1,0:T(8,128)(2,1)S(1)} %fusion.11, s32[]{:T(128)S(6)} %select_n.19), kind=kOutput, calls=%fused_computation.25 | convolution fusion | flops 2097152 | bytes 282628 | tf_op jit(solution)/shard_map/dot_general | solution.py:45
  20.6 1.1 %fusion.13 = f32[8,128]{1,0:T(8,128)S(1)} fusion(bf16[1024,128]{1,0:T(8,128)(2,1)} %param.17, bf16[8,4096]{1,0:T(8,128)(2,1)S(1)} %fusion.11, s32[]{:T(128)S(6)} %select_n.19), kind=kOutput, calls=%fused_computation.23 | convolution fusion | flops 2097152 | bytes 282628 | tf_op jit(solution)/shard_map/dot_general | solution.py:46
  21.7 0.4 fusion.17
  22.0 19.1 %psum.35 = bf16[8,1024]{1,0:T(8,128)(2,1)S(1)} all-reduce(f32[8,1024]{1,0:T(8,128)S(1)} %fusion.17), channel_id=1, replica_groups=mesh['grp'=2,'kv'=4,'tp'=4] {'kv'}, use_global_device_ids=true, to_apply=%region_1.0 | all-reduce | flops 8192 | bytes 49152 | tf_op jit(solution)/shard_map/psum | solution.py:47
  41.2 0.1 reshape.76
  41.3 2.7 %copy.18 = bf16[8,768,128]{1,2,0:T(8,128)(2,1)} copy(bf16[8,768,128]{2,1,0:T(8,128)(2,1)} %param.21) | data formatting | bytes 3145728 | tf_op args[8]
  43.9 1.8 %fusion.33 = (f32[8,2,8]{2,1,0:T(2,128)S(1)}, f32[8,2,8,768]{3,2,1,0:T(8,128)S(1)}) fusion(f32[8,16,768]{2,1,0:T(8,128)S(1)} %copy-done.1, f32[8,16]{1,0:T(8,128)S(1)} %fusion.22, bf16[8,2,8,64]{3,2,1,0:T(8,128)(2,1)S(1)} %reshape.76, bf16[8,768,2,64]{1,3,2,0:T(8,128)(2,1)} %bitcast.26, pred[8,768]{1,0:T(8,128)(4,1)S(1)} %broadcast_compare_fusion), kind=kOutput, calls=%fused_computation.45 | convolution fusion | flops 13074304 | bytes 2382848 | tf_op jit(solution)/shard_map/skgd,spkd->skgp/dot_general | solution.py:61
  45.7 8.5 %pmax.7 = f32[8,2,8]{2,1,0:T(2,128)S(1)} all-reduce(f32[8,2,8]{2,1,0:T(2,128)S(1)} %get-tuple-element.12), channel_id=1, replica_groups=mesh['grp'=2,'kv'=4,'tp'=4] {'kv'}, use_global_device_ids=true, to_apply=%region_3.0 | all-reduce | flops 128 | bytes 1024 | tf_op jit(solution)/shard_map/pmax | solution.py:81
  54.3 0.2 fusion.3
  54.5 2.6 %copy.19 = bf16[8,768,128]{1,2,0:T(8,128)(2,1)} copy(bf16[8,768,128]{2,1,0:T(8,128)(2,1)} %param.22) | data formatting | bytes 3145728 | tf_op args[9]
  57.1 2.0 %convolution_multiply_fusion.1 = f32[8,2,8,64]{3,2,1,0:T(8,128)S(1)} fusion(bf16[8,768,2,64]{1,3,2,0:T(8,128)(2,1)} %bitcast.27, f32[8,2,8,768]{3,2,1,0:T(8,128)S(1)} %get-tuple-element.13, f32[8,2,8]{2,1,0:T(2,128)S(1)} %get-tuple-element.12, pred[8,768]{1,0:T(8,128)(4,1)S(1)} %broadcast_compare_fusion, f32[8,2,8]{2,1,0:T(2,128)S(1)} %bitcast.32), kind=kOutput, calls=%fused_computation.3 | convolution fusion | flops 12886016 | bytes 2006016 | tf_op jit(solution)/shard_map/skgp,spkd->skgd/dot_general | solution.py:75
  59.1 18.7 %all-reduce = (f32[8,2,8,64]{3,2,1,0:T(8,128)S(1)}, bf16[8,128]{1,0:T(8,128)(2,1)S(1)}, f32[8,2,8]{2,1,0:T(2,128)S(1)}, bf16[8,128]{1,0:T(8,128)(2,1)S(1)}) all-reduce(f32[8,2,8,64]{3,2,1,0:T(8,128)S(1)} %convolution_multiply_fusion.1, f32[8,128]{1,0:T(8,128)S(1)} %fusion.15, ...), channel_id=1, replica_groups=mesh['grp'=2,'kv'=4,'tp'=4] {'kv'}, use_global_device_ids=true, to_apply=%region_4.5 | all-reduce | flops 10368 | bytes 78848 | tf_op jit(solution)/shard_map/psum | solution.py:83
  77.9 0.1 fusion.34
  78.1 0.1 divide_convert_fusion
  78.3 0.1 convert_element_type.51
  78.4 2.2 %convolution_convert_fusion = bf16[8,1024]{1,0:T(8,128)(2,1)S(1)} fusion(bf16[8,1024]{1,0:T(8,128)(2,1)S(1)} %convert_element_type.51, bf16[1024,1024]{1,0:T(8,128)(2,1)} %param.20), kind=kOutput, calls=%fused_computation.4 | convolution fusion | flops 16785408 | bytes 2129920 | tf_op jit(solution)/shard_map/dot_general | solution.py:104
  80.6 5.2 %all-gather = bf16[32,1024]{1,0:T(8,128)(2,1)S(1)} all-gather(bf16[8,1024]{1,0:T(8,128)(2,1)S(1)} %convolution_convert_fusion), channel_id=2, replica_groups=mesh['grp'=2,'kv'=4,'tp'=4] {'tp'}, dimensions={0}, use_global_device_ids=true | all-gather | bytes 81920 | tf_op jit(solution)/shard_map/all_gather | solution.py:108
  85.8 0.6 bitcast_reduce_fusion
  (14 shorter events, 0.2 us)
Async XLA Ops:
  0.6 21.0 %copy-start = (bf16[1024,1024]{1,0:T(8,128)(2,1)S(1)}, bf16[1024,1024]{1,0:T(8,128)(2,1)}, u32[]{:S(2)}) copy-start(bf16[1024,1024]{1,0:T(8,128)(2,1)} %param.15) | copy-start | bytes 6291460
  41.3 2.7 %copy-start.1 = (f32[8,16,768]{2,1,0:T(8,128)S(1)}, f32[8,16,768]{2,1,0:T(8,128)}, u32[]{:S(2)}) copy-start(f32[8,16,768]{2,1,0:T(8,128)} %param.23) | copy-start | bytes 1179652
  77.8 8.7 %copy-start.2 = (bf16[8,128]{1,0:T(8,128)(2,1)}, bf16[8,128]{1,0:T(8,128)(2,1)S(1)}, u32[]{:S(2)}) copy-start(bf16[8,128]{1,0:T(8,128)(2,1)S(1)} %get-tuple-element.4) | copy-start | bytes 6148
  77.8 8.7 %copy-start.3 = (bf16[8,128]{1,0:T(8,128)(2,1)}, bf16[8,128]{1,0:T(8,128)(2,1)S(1)}, u32[]{:S(2)}) copy-start(bf16[8,128]{1,0:T(8,128)(2,1)S(1)} %get-tuple-element.6) | copy-start | bytes 6148
